TPU v7x, 32 devices: a whole 2x2x4 slice. The times are simulated.
32 devices in a mesh: kv: 8 (over z, x), tp: 4 (over y, core).
Axes of the slice: x: 2, y: 2, z: 4, core: 2. Of those that a mesh axis runs over, the one named last changes fastest.
Arguments:
- tokens: bfloat16 [16384, 2048], P('kv'), may hold values from -6 to 6
- norm_gain: bfloat16 [2048], replicated, may hold values from 0.099609375 to 1.8984375
- query_weight: bfloat16 [2048, 1024], P(None, 'tp'), may hold values from -0.125 to 0.125
- cmp_key_weight: bfloat16 [2048, 512], P(None, 'tp'), may hold values from -0.125 to 0.125
- cmp_value_weight: bfloat16 [2048, 512], P(None, 'tp'), may hold values from -0.125 to 0.125
- sel_key_weight: bfloat16 [2048, 512], P(None, 'tp'), may hold values from -0.125 to 0.125
- sel_value_weight: bfloat16 [2048, 512], P(None, 'tp'), may hold values from -0.125 to 0.125
- branch_weight: bfloat16 [2, 2048, 16], replicated, may hold values from -0.125 to 0.125
- key_embed: bfloat16 [8, 32, 64], P('tp'), may hold values from -3 to 3
- key_inner: bfloat16 [8, 2048, 64], P('tp'), may hold values from -0.125 to 0.125
- key_outer: bfloat16 [8, 64, 64], P('tp'), may hold values from -0.75 to 0.75
- value_embed: bfloat16 [8, 32, 64], P('tp'), may hold values from -3 to 3
- value_inner: bfloat16 [8, 2048, 64], P('tp'), may hold values from -0.125 to 0.125
- value_outer: bfloat16 [8, 64, 64], P('tp'), may hold values from -0.75 to 0.75
- out_weight: bfloat16 [1024, 2048], replicated, may hold values from -0.1875 to 0.1875
- chosen: int32 [8, 128, 8], P('tp'), may hold values from 0 to 255, as said below
Outputs:
- attended: bfloat16 [16384, 2048], P(('kv', 'tp'))
Inputs may be any that keep to these rules, and one draw needn't show every extreme that they name: `chosen`: each entry is the index of a block of 64 positions in the whole sequence. For every key head and query block, its 8 entries lie in 8 different aligned spans of 2048 positions (at most one from any span), and none lies inside the query block's own positions.
All inputs are finite; a program needn't handle non-finite values.
Results may differ from a plain program's by a relative error of at most 0.0075.
Values may be sent and summed in bfloat16 or wider, within the bound.
A program may use at most 128 MiB of HBM per device.

v0:
```python
import jax
import jax.numpy as jnp
from jax import lax
from jax.sharding import PartitionSpec as P

HEAD_DIM = 64
CMP_BLOCK = 32
SEL_BLOCK = 64
Q_BLOCK = 128
FAR_PICKS = 8
ROPE_BASE = 10000.0
norm_eps = 1e-06
masked_score = -1000000000.0


def rotate(values_in, positions):
    half_dim = values_in.shape[-1] // 2
    inverse = ROPE_BASE ** (-jnp.arange(half_dim, dtype=jnp.float32) / half_dim)
    rotary_phases = positions.astype(jnp.float32)[:, None] * inverse[None, :]
    cosine = jnp.cos(rotary_phases)[:, None, :]
    sine = jnp.sin(rotary_phases)[:, None, :]
    first_half = values_in[..., :half_dim]
    second_half = values_in[..., half_dim:]
    return jnp.concatenate(
        [first_half * cosine - second_half * sine, second_half * cosine + first_half * sine],
        axis=-1,
    )


def summarize(raw_rows, embed, inner, outer):
    kv_local = embed.shape[0]
    block_count = raw_rows.shape[0] // CMP_BLOCK
    blocked = (
        raw_rows.reshape(block_count, CMP_BLOCK, kv_local, HEAD_DIM)
        .transpose(2, 0, 1, 3)
        .astype(jnp.float32)
    )
    blocked = (blocked + embed.astype(jnp.float32)[:, None]).astype(jnp.bfloat16)
    blocked = blocked.reshape(kv_local, block_count, CMP_BLOCK * HEAD_DIM)
    hidden = jax.nn.gelu(
        jnp.einsum("knc,kce->kne", blocked, inner, preferred_element_type=jnp.float32)
    ).astype(jnp.bfloat16)
    return jnp.einsum("kne,kef->knf", hidden, outer, preferred_element_type=jnp.float32).astype(
        jnp.bfloat16
    )


def per_device(
    tokens,
    norm_gain,
    query_weight,
    cmp_key_weight,
    cmp_value_weight,
    sel_key_weight,
    sel_value_weight,
    branch_weight,
    key_embed,
    key_inner,
    key_outer,
    value_embed,
    value_inner,
    value_outer,
    out_weight,
    chosen,
):
    tok_rows = tokens.shape[0]
    kv_local = key_embed.shape[0]
    heads_local = query_weight.shape[1] // HEAD_DIM
    group_size = heads_local // kv_local
    owners = lax.axis_size("kv")
    dev_index = lax.axis_index("kv")
    offset = dev_index * tok_rows
    positions = offset + jnp.arange(tok_rows, dtype=jnp.int32)
    scale = HEAD_DIM ** (-0.5)
    expanded_mask = tokens.astype(jnp.float32)
    normed = (
        expanded_mask
        * lax.rsqrt(jnp.mean(expanded_mask * expanded_mask, axis=-1, keepdims=True) + norm_eps)
        * norm_gain.astype(jnp.float32)
    ).astype(jnp.bfloat16)
    gate_cols = lax.dynamic_slice_in_dim(
        branch_weight, lax.axis_index("tp") * heads_local, heads_local, 2
    )
    q_width = heads_local * HEAD_DIM
    kv_width = kv_local * HEAD_DIM
    joined_weight = jnp.concatenate(
        [
            query_weight,
            cmp_key_weight,
            cmp_value_weight,
            sel_key_weight,
            sel_value_weight,
            gate_cols[0],
            gate_cols[1],
        ],
        axis=1,
    )
    projected = jnp.dot(normed, joined_weight, preferred_element_type=jnp.float32)
    bounds = [
        q_width,
        q_width + kv_width,
        q_width + 2 * kv_width,
        q_width + 3 * kv_width,
        q_width + 4 * kv_width,
        q_width + 4 * kv_width + heads_local,
    ]
    (
        query_part,
        cmp_key_part,
        cmp_value_part,
        sel_key_part,
        sel_value_part,
        gate_cmp_part,
        gate_sel_part,
    ) = jnp.split(projected, bounds, axis=1)
    query = query_part.reshape(tok_rows, heads_local, HEAD_DIM)
    q_plain = query.astype(jnp.bfloat16)
    q_turn = rotate(query, positions).astype(jnp.bfloat16)
    cmp_key = cmp_key_part.astype(jnp.bfloat16).reshape(tok_rows, kv_local, HEAD_DIM)
    cmp_value = cmp_value_part.astype(jnp.bfloat16).reshape(tok_rows, kv_local, HEAD_DIM)
    sel_key = rotate(sel_key_part.reshape(tok_rows, kv_local, HEAD_DIM), positions).astype(
        jnp.bfloat16
    )
    selected_value = sel_value_part.astype(jnp.bfloat16).reshape(tok_rows, kv_local, HEAD_DIM)
    gate_cmp = jax.nn.sigmoid(gate_cmp_part)
    gate_sel = jax.nn.sigmoid(gate_sel_part)
    summary = jnp.concatenate(
        [
            summarize(cmp_key, key_embed, key_inner, key_outer),
            summarize(cmp_value, value_embed, value_inner, value_outer),
        ],
        axis=-1,
    )
    summaries = lax.all_gather(summary, "kv", axis=1, tiled=True)
    summary_count = summaries.shape[1]
    block_end = (jnp.arange(summary_count, dtype=jnp.int32) + 1) * CMP_BLOCK - 1
    q_group = q_plain.reshape(tok_rows, kv_local, group_size, HEAD_DIM).transpose(1, 0, 2, 3)
    cmp_scores = (
        jnp.einsum(
            "ktgd,kcd->ktgc", q_group, summaries[..., :HEAD_DIM], preferred_element_type=jnp.float32
        )
        * scale
    )
    usable = (block_end[None, :] <= positions[:, None])[None, :, None, :]
    cmp_probs = jax.nn.softmax(
        jnp.where(usable, cmp_scores, masked_score), axis=-1
    ) * usable.astype(jnp.float32)
    out_cmp = jnp.einsum(
        "ktgc,kcd->ktgd",
        cmp_probs.astype(jnp.bfloat16),
        summaries[..., HEAD_DIM:],
        preferred_element_type=jnp.float32,
    )
    out_cmp = out_cmp.transpose(1, 0, 2, 3).reshape(tok_rows, heads_local, HEAD_DIM)
    span_queries = tok_rows // Q_BLOCK
    kv_sel = jnp.concatenate([sel_key, selected_value], axis=-1).transpose(1, 0, 2)
    all_picks = chosen.reshape(kv_local, owners, span_queries, FAR_PICKS)
    my_picks = lax.dynamic_index_in_dim(all_picks, dev_index, 1, keepdims=False)
    head_lane = jnp.arange(kv_local, dtype=jnp.int32)[:, None, None]
    empty = jnp.zeros((kv_local, span_queries, FAR_PICKS, SEL_BLOCK, 2 * HEAD_DIM), jnp.bfloat16)
    piece = lax.all_gather(kv_sel, "kv", axis=1, tiled=True)
    block_count = piece.shape[1] // SEL_BLOCK
    blocked = piece.reshape(kv_local, block_count, SEL_BLOCK, 2 * HEAD_DIM)
    inside = (my_picks >= 0) & (my_picks < block_count)
    clipped = jnp.clip(my_picks, 0, block_count - 1)
    fetched = blocked[head_lane, clipped]
    picked = jnp.where(inside[..., None, None], fetched, empty)
    own_keys = kv_sel.reshape(kv_local, span_queries, Q_BLOCK, 2 * HEAD_DIM)
    keys_all = jnp.concatenate(
        [own_keys, picked.reshape(kv_local, span_queries, FAR_PICKS * SEL_BLOCK, 2 * HEAD_DIM)],
        axis=2,
    )
    query_pos = positions.reshape(span_queries, Q_BLOCK)
    far_pos = (my_picks[..., None] * SEL_BLOCK + jnp.arange(SEL_BLOCK, dtype=jnp.int32)).reshape(
        kv_local, span_queries, FAR_PICKS * SEL_BLOCK
    )
    key_pos = jnp.concatenate(
        [jnp.broadcast_to(query_pos[None], (kv_local, span_queries, Q_BLOCK)), far_pos], axis=2
    )
    q_sel = q_turn.reshape(span_queries, Q_BLOCK, kv_local, group_size, HEAD_DIM).transpose(
        2, 0, 1, 3, 4
    )
    sel_scores = (
        jnp.einsum(
            "knqgd,knmd->knqgm", q_sel, keys_all[..., :HEAD_DIM], preferred_element_type=jnp.float32
        )
        * scale
    )
    allowed_keys = key_pos[:, :, None, None, :] <= query_pos[None, :, :, None, None]
    sel_probs = jax.nn.softmax(jnp.where(allowed_keys, sel_scores, masked_score), axis=-1)
    out_sel = jnp.einsum(
        "knqgm,knmd->knqgd",
        sel_probs.astype(jnp.bfloat16),
        keys_all[..., HEAD_DIM:],
        preferred_element_type=jnp.float32,
    )
    out_sel = out_sel.transpose(1, 2, 0, 3, 4).reshape(tok_rows, heads_local, HEAD_DIM)
    mixed = (
        (gate_cmp[..., None] * out_cmp + gate_sel[..., None] * out_sel)
        .reshape(tok_rows, heads_local * HEAD_DIM)
        .astype(jnp.bfloat16)
    )
    head_rows = lax.all_to_all(mixed, "tp", split_axis=0, concat_axis=1, tiled=True)
    return jnp.dot(head_rows, out_weight, preferred_element_type=jnp.float32).astype(jnp.bfloat16)


def solution(mesh):
    placed = (
        P("kv", None),
        P(),
        P(None, "tp"),
        P(None, "tp"),
        P(None, "tp"),
        P(None, "tp"),
        P(None, "tp"),
        P(),
        P("tp", None, None),
        P("tp", None, None),
        P("tp", None, None),
        P("tp", None, None),
        P("tp", None, None),
        P("tp", None, None),
        P(),
        P("tp", None, None),
    )
    return jax.shard_map(
        per_device, mesh=mesh, in_specs=placed, out_specs=P(("kv", "tp"), None), check_vma=False
    )
```

profile of v0, /device:TPU:0, one launch (start us, length us, event | category | flops | bytes accessed | tf_op | source)
XLA Modules:
  0.0 275.9 jit_solution(4170866323818475863)
XLA Ops:
  7.3 5.1 %fusion.2 = f32[2048]{0:T(1024)S(1)} fusion(bf16[2048,2048]{1,0:T(8,128)(2,1)} %param.16), kind=kLoop, calls=%fused_computation.8 | loop fusion | flops 12580864 | bytes 8396800 | tf_op jit(solution)/shard_map/reduce_sum | solution.py:78
  14.9 1.3 copy.114
  16.2 1.3 copy.116
  17.5 6.6 %concatenate.30 = bf16[2048,776]{1,0:T(8,128)(2,1)} concatenate(bf16[2048,256]{1,0:T(8,128)(2,1)S(1)} %copy-done.6, bf16[2048,128]{1,0:T(8,128)(2,1)} %param.19, bf16[2048,128]{1,0:T(8,128)(2,1)} %param.20, bf16[2048,128]{1,0:T(8,128)(2,1)} %param.21, bf16[2048,128]{1,0:T(8,128)(2,1)} %param.22, bf16[2048,4]{1,0:T(8,128)(2,1)S(1)} %copy.101, bf16[2048,4]{1,0:T(8,128)(2,1)S(1)} %copy.102), dimensions={1} | concatenate | bytes 6356992 | tf_op jit(solution)/shard_map/concatenate | solution.py:86
  24.2 12.3 %fusion.89 = (bf16[2048,776]{0,1:T(8,128)(2,1)S(1)}, f32[2048,776]{0,1:T(8,128)}) fusion(bf16[2048,776]{1,0:T(8,128)(2,1)} %concatenate.30, bf16[2048,2048]{1,0:T(8,128)(2,1)} %param.16, f32[2048]{0:T(1024)S(1)} %convert_element_type.94, f32[2048]{0:T(1024)S(1)} %add_rsqrt_fusion), kind=kOutput, calls=%fused_computation.134 | convolution fusion | flops 6527926272 | bytes 21118976 | tf_op jit(solution)/shard_map/dot_general | solution.py:98
  36.5 1.5 slice_convert_fusion.1
  38.5 1.3 split.36
  39.9 1.9 copy.135
  41.9 2.0 copy.134
  43.8 3.3 %subtract_convert_fusion = (bf16[2048,2,32]{2,0,1:T(8,128)(2,1)S(1)}, bf16[2048,2,32]{2,0,1:T(8,128)(2,1)S(1)}) fusion(f32[2048,2,32]{2,0,1:T(8,128)} %copy.135, f32[2048,2,32]{2,0,1:T(8,128)} %copy.134, f32[2048,32]{1,0:T(8,128)} %copy.116, f32[2048,32]{1,0:T(8,128)} %copy.114), kind=kLoop, calls=%fused_computation.45 | loop fusion | flops 1048576 | bytes 2097152 | tf_op jit(solution)/shard_map/convert.5
  47.2 1.1 copy-done.2
  48.2 2.0 fusion.107
  50.3 2.8 %split.55 = bf16[2048,256]{0,1:T(8,128)(2,1)} slice(f32[2048,776]{0,1:T(8,128)} %get-tuple-element.25), slice={[0:2048], [0:256]} | slice | bytes 2097152 | tf_op jit(solution)/shard_map/split | solution.py:115
  53.1 3.1 %split.34 = f32[2048,256]{0,1:T(8,128)} slice(f32[2048,776]{0,1:T(8,128)} %get-tuple-element.25), slice={[0:2048], [0:256]} | slice | bytes 4194304 | tf_op jit(solution)/shard_map/split | solution.py:115
  57.3 2.6 copy.103
  59.8 3.5 %reshape.279 = f32[64,32,2,64]{3,2,1,0:T(2,128)} reshape(f32[2048,128]{1,0:T(8,128)} %copy.103) | data formatting | bytes 2097152 | tf_op jit(solution)/shard_map/convert_element_type | solution.py:36
  63.3 2.8 %fusion.28 = bf16[2,64,32,64]{3,2,1,0:T(8,128)(2,1)} fusion(f32[64,32,2,64]{3,2,1,0:T(2,128)} %reshape.279, f32[2,32,64]{2,1,0:T(8,128)S(1)} %convert_element_type.101), kind=kLoop, calls=%fused_computation.42 | loop fusion | flops 524288 | bytes 1589248 | tf_op jit(solution)/shard_map/convert_element_type | solution.py:38
  66.1 2.7 reshape.269
  68.8 2.5 copy.105
  71.4 3.4 %reshape.280 = f32[64,32,2,64]{3,2,1,0:T(2,128)} reshape(f32[2048,128]{1,0:T(8,128)} %copy.105) | data formatting | bytes 2097152 | tf_op jit(solution)/shard_map/convert_element_type | solution.py:36
  74.8 2.8 %fusion.27 = bf16[2,64,32,64]{3,2,1,0:T(8,128)(2,1)} fusion(f32[64,32,2,64]{3,2,1,0:T(2,128)} %reshape.280, f32[2,32,64]{2,1,0:T(8,128)S(1)} %convert_element_type.108), kind=kLoop, calls=%fused_computation.40 | loop fusion | flops 524288 | bytes 1589248 | tf_op jit(solution)/shard_map/convert_element_type | solution.py:38
  77.5 15.1 %reshape.270 = bf16[2,64,2048]{2,1,0:T(8,128)(2,1)} reshape(bf16[2,64,32,64]{3,2,1,0:T(8,128)(2,1)} %fusion.27) | data formatting | bytes 1048576 | tf_op jit(solution)/shard_map/reshape | solution.py:39
  92.7 1.8 subtract_convert_fusion.1
  96.8 1.6 mul.206
  98.3 3.7 %mul.207 = f32[4,512,256]{1,0,2:T(4,128)} reshape(f32[2048,4,64]{0,2,1:T(8,128)} %mul.206) | data formatting | bytes 4194304 | tf_op jit(solution)/shard_map/mul | solution.py:199
  102.0 3.2 %pad_maximum_fusion.1 = bf16[2048,2,128]{2,0,1:T(8,128)(2,1)} fusion(bf16[2048,2,64]{2,0,1:T(8,128)(2,1)S(1)} %copy.117, bf16[2048,2,32]{2,0,1:T(8,128)(2,1)} %copy-done.2, bf16[2048,2,32]{2,0,1:T(8,128)(2,1)S(1)} %get-tuple-element.7), kind=kLoop, calls=%fused_computation.54 | loop fusion | flops 3145728 | bytes 2097152 | tf_op jit(solution)/shard_map/concatenate | solution.py:156
  105.2 2.3 copy.121
  107.7 2.4 mul.225
  110.2 1.5 convolution_convert_fusion.2
  111.7 1.6 convolution_convert_fusion.1
  113.5 35.5 %all_gather.6 = bf16[2,512,128]{2,1,0:T(8,128)(2,1)S(1)} all-gather(bf16[2,64,128]{2,1,0:T(8,128)(2,1)S(1)} %pad_maximum_fusion.2), channel_id=1, replica_groups=mesh['kv'=8,'tp'=4] {'kv'}, dimensions={1}, use_global_device_ids=true | all-gather | bytes 294912 | tf_op jit(solution)/shard_map/all_gather | solution.py:134
  149.0 2.7 fusion.87
  151.7 9.7 %fusion.91 = (f32[2,2048,2]{1,2,0:T(2,128)S(1)}, f32[2,2048,2,512]{1,3,2,0:T(8,128)}) fusion(pred[2048,512]{0,1:T(8,128)(4,1)S(1)} %get-tuple-element.21, bf16[2,2048,2,64]{1,3,2,0:T(8,128)(2,1)S(1)} %bitcast.127, bf16[2,512,128]{2,1,0:T(8,128)(2,1)S(1)} %all_gather.6), kind=kOutput, calls=%fused_computation.136 | convolution fusion | flops 553648640 | bytes 19169280 | tf_op jit(solution)/shard_map/sub | solution.py:145
  161.4 8.2 %fusion.19 = f32[2048,2,2,64]{0,3,2,1:T(8,128)S(1)} fusion(f32[2,2048,2,512]{1,3,2,0:T(8,128)} %get-tuple-element.29, f32[2048,512]{0,1:T(8,128)} %get-tuple-element.20, f32[2,2048,2]{1,2,0:T(2,128)S(1)} %get-tuple-element.28, bf16[2,512,128]{2,1,0:T(8,128)(2,1)S(1)} %all_gather.6), kind=kOutput, calls=%fused_computation.32 | convolution fusion | flops 549453824 | bytes 23363584 | tf_op jit(solution)/shard_map/ktgc,kcd->ktgd/dot_general | solution.py:148
  169.6 2.4 reshape.271
  172.0 2.7 broadcast_compare_fusion
  174.7 7.8 %all-gather.2.cloned.1.call-done = bf16[2,16384,128]{2,1,0:T(8,128)(2,1)} async-done(((bf16[2,2048,128]{2,1,0:T(8,128)(2,1)}), bf16[2,16384,128]{2,1,0:T(8,128)(2,1)}) %all-gather.2.cloned.1.call-update) | async-done | bytes 8388624 | tf_op jit(solution)/shard_map/all_gather | solution.py:161
  182.5 6.7 %gather_fusion = bf16[256,64,128]{2,1,0:T(8,128)(2,1)} fusion(bf16[2,256,64,128]{3,2,1,0:T(8,128)(2,1)} %bitcast.123, s32[256]{0:T(256)S(1)} %reshape.281), kind=kCustom, calls=%fused_computation | custom fusion | bytes 8390656 | tf_op jit(solution)/shard_map/gather | solution.py:166
  189.2 6.3 %copy.120 = bf16[2,16,512,128]{2,3,1,0:T(8,128)(2,1)} copy(bf16[2,16,512,128]{3,2,1,0:T(8,128)(2,1)} %bitcast.117) | data formatting | bytes 8388608 | tf_op jit(solution)/shard_map/gather | solution.py:166
  195.5 2.6 broadcast_select_fusion
  198.2 8.6 %fusion.22 = f32[2,16,128,2,640]{4,2,3,1,0:T(8,128)} fusion(bf16[2,16,128,128]{2,3,1,0:T(8,128)(2,1)S(1)} %copy-done.3, bf16[2,16,512,128]{2,3,1,0:T(8,128)(2,1)S(1)} %broadcast_select_fusion, bf16[16,128,2,2,32]{1,4,3,0,2:T(8,128)(2,1)S(1)} %copy-done.5, bf16[16,128,2,2,32]{1,4,3,0,2:T(8,128)(2,1)S(1)} %copy.111), kind=kOutput, calls=%fused_computation.35 | convolution fusion | flops 678428672 | bytes 27262976 | tf_op jit(solution)/shard_map/knqgd,knmd->knqgm/dot_general | solution.py:184
  206.7 24.3 %fusion.90 = (f32[2,16,128,2]{2,3,1,0:T(2,128)S(1)}, f32[2,16,128,2,640]{4,2,3,1,0:T(8,128)}) fusion(f32[2,16,128,2,640]{4,2,3,1,0:T(8,128)} %fusion.22, pred[2,16,128,640]{3,2,1,0:T(8,128)(4,1)S(1)} %copy-done.4), kind=kOutput, calls=%fused_computation.135 | output fusion | flops 31457920 | bytes 44597248 | tf_op jit(solution)/shard_map/sub | solution.py:190
  231.1 9.1 %fusion.31 = f32[16,128,2,2,64]{1,4,3,0,2:T(8,128)S(1)} fusion(bf16[2,16,512,128]{2,3,1,0:T(8,128)(2,1)S(1)} %broadcast_select_fusion, bf16[2,16,128,128]{2,3,1,0:T(8,128)(2,1)S(1)} %copy-done.3, f32[2,16,128,2,640]{4,2,3,1,0:T(8,128)} %get-tuple-element.27, f32[2,16,128,2]{2,3,1,0:T(2,128)S(1)} %get-tuple-element.26), kind=kOutput, calls=%fused_computation.48 | convolution fusion | flops 686817280 | bytes 28344320 | tf_op jit(solution)/shard_map/knqgm,knmd->knqgd/dot_general | solution.py:191
  240.1 1.2 copy.122
  241.4 1.7 reshape.278
  243.1 4.5 %add_convert_fusion = bf16[4,512,256]{1,0,2:T(4,128)(2,1)S(1)} fusion(f32[4,512,256]{1,0,2:T(4,128)} %mul.225, f32[4,512,256]{1,0,2:T(4,128)} %reshape.278, f32[4,512,256]{1,0,2:T(4,128)} %mul.207, f32[4,512,256]{1,0,2:T(4,128)} %reshape.271), kind=kLoop, calls=%fused_computation.43 | loop fusion | flops 2097152 | bytes 9437184 | tf_op jit(solution)/shard_map/convert_element_type | solution.py:201
  247.9 17.2 %all_to_all.16 = bf16[4,512,256]{1,2,0:T(8,128)(2,1)S(1)} all-to-all(bf16[4,512,256]{1,2,0:T(8,128)(2,1)S(1)} %copy.123), channel_id=1, replica_groups=mesh['kv'=8,'tp'=4] {'tp'}, dimensions={0} | all-to-all | bytes 2097152 | tf_op jit(solution)/shard_map/all_to_all | solution.py:203
  265.1 3.8 %convolution_convert_fusion = bf16[512,2048]{1,0:T(8,128)(2,1)} fusion(bf16[512,1024]{0,1:T(8,128)(2,1)S(1)} %bitcast.128, bf16[1024,2048]{1,0:T(8,128)(2,1)S(1)} %copy-done.11), kind=kOutput, calls=%fused_computation.31 | convolution fusion | flops 2148532224 | bytes 7340032 | tf_op jit(solution)/shard_map/dot_general | solution.py:204
  (68 shorter events, 7.6 us)
Async XLA Ops:
  6.5 103.6 %copy-start = (bf16[2,2048,64]{1,2,0:T(8,128)(2,1)S(1)}, bf16[2,2048,64]{1,2,0:T(8,128)(2,1)}, u32[]{:S(2)}) copy-start(bf16[2,2048,64]{1,2,0:T(8,128)(2,1)} %param.25) | copy-start | bytes 1572868
  6.5 176.0 %all-gather.2.cloned.1.call-start = ((), (), s32[]{:S(2)}) async-start(), calls=%async_computation.1 | async-start | bytes 9437184 | tf_op jit(solution)/shard_map/all_gather | solution.py:161
  12.4 5.2 %copy-start.6 = (bf16[2048,256]{1,0:T(8,128)(2,1)S(1)}, bf16[2048,256]{1,0:T(8,128)(2,1)}, u32[]{:S(2)}) copy-start(bf16[2048,256]{1,0:T(8,128)(2,1)} %param.18) | copy-start | bytes 3145732
  47.2 1.1 copy-start.2
  50.2 6.1 %copy-start.8 = (bf16[2,32,64]{2,1,0:T(8,128)(2,1)S(1)}, bf16[2,32,64]{2,1,0:T(8,128)(2,1)}, u32[]{:S(2)}) copy-start(bf16[2,32,64]{2,1,0:T(8,128)(2,1)} %param.24) | copy-start | bytes 24580
  50.2 6.1 %copy-start.9 = (bf16[2,32,64]{2,1,0:T(8,128)(2,1)S(1)}, bf16[2,32,64]{2,1,0:T(8,128)(2,1)}, u32[]{:S(2)}) copy-start(bf16[2,32,64]{2,1,0:T(8,128)(2,1)} %param.27) | copy-start | bytes 24580
  50.2 6.1 %copy-start.10 = (s32[2,128,8]{1,2,0:T(8,128)S(1)}, s32[2,128,8]{1,2,0:T(8,128)}, u32[]{:S(2)}) copy-start(s32[2,128,8]{1,2,0:T(8,128)} %param.31) | copy-start | bytes 24580
  105.2 5.0 %copy-start.12 = (bf16[2,64,64]{2,1,0:T(8,128)(2,1)S(1)}, bf16[2,64,64]{2,1,0:T(8,128)(2,1)}, u32[]{:S(2)}) copy-start(bf16[2,64,64]{2,1,0:T(8,128)(2,1)} %param.26) | copy-start | bytes 49156
  107.5 4.2 %copy-start.13 = (bf16[2,64,64]{2,1,0:T(8,128)(2,1)S(1)}, bf16[2,64,64]{2,1,0:T(8,128)(2,1)}, u32[]{:S(2)}) copy-start(bf16[2,64,64]{2,1,0:T(8,128)(2,1)} %param.29) | copy-start | bytes 49156
  110.2 41.6 %copy-start.7 = (bf16[2048,256]{0,1:T(8,128)(2,1)S(1)}, bf16[2048,256]{0,1:T(8,128)(2,1)}, u32[]{:S(2)}) copy-start(bf16[2048,256]{0,1:T(8,128)(2,1)} %split.55) | copy-start | bytes 3145732
  195.5 2.6 copy-start.3
  195.5 2.7 copy-start.5
  198.2 8.6 %copy-start.4 = (pred[2,16,128,640]{3,2,1,0:T(8,128)(4,1)S(1)}, pred[2,16,128,640]{3,2,1,0:T(8,128)(4,1)}, u32[]{:S(2)}) copy-start(pred[2,16,128,640]{3,2,1,0:T(8,128)(4,1)} %broadcast_compare_fusion) | copy-start | bytes 7864324
  247.6 17.5 %copy-start.11 = (bf16[1024,2048]{1,0:T(8,128)(2,1)S(1)}, bf16[1024,2048]{1,0:T(8,128)(2,1)}, u32[]{:S(2)}) copy-start(bf16[1024,2048]{1,0:T(8,128)(2,1)} %param.30) | copy-start | bytes 12582916
  265.1 3.8 %copy-start.1 = (bf16[2,2048,64]{1,2,0:T(8,128)(2,1)S(1)}, bf16[2,2048,64]{1,2,0:T(8,128)(2,1)}, u32[]{:S(2)}) copy-start(bf16[2,2048,64]{1,2,0:T(8,128)(2,1)} %param.25) | copy-start | bytes 1572868
Sparse Core Ops, SparseCore 0:
  50.4 132.0 all-gather.1
where the time goes:
time: 280 us; the launch traced here: 276 us
  local copies, waits for them, and re-layouts  84.3 us (30%)
  other arithmetic  62.4 us (22%)
  matrix products  54.7 us (20%)
  blocking collectives  52.8 us (19%)
  between operations  13.9 us (5%)
  waiting for transfers between devices  7.81 us (3%)
    all_gather x1, blocking collectives, per_device(): summaries = lax.all_gather(summary, 'kv', axis=1, tiled=True)  35.5 us
    sub x1, other arithmetic, per_device(): jax.nn.softmax(jnp.where(allowed_keys, sel_scores, masked_score), axis=-1)  24.3 us
    reshape x2, local copies, waits for them, and re-layouts, summarize(): blocked = blocked.reshape(kv_local, block_count, CMP_BLOCK * HEAD_DIM)  17.8 us
    all_to_all x1, blocking collectives, per_device(): lax.all_to_all(mixed, 'tp', split_axis=0, concat_axis=1, tiled=True)  17.2 us
    gather x2, local copies, waits for them, and re-layouts, per_device(): fetched = blocked[head_lane, clipped]  13 us
    dot_general x1, matrix products, per_device(): jnp.dot(normed, joined_weight, preferred_element_type=jnp.float32)  12.3 us
    convert_element_type x4, local copies, waits for them, and re-layouts, summarize(): blocked = raw_rows.reshape(block_count, CMP_BLOCK, kv_local, HEAD_DIM).tr...  12 us
    sub x1, matrix products, per_device(): jax.nn.softmax(jnp.where(usable, cmp_scores, masked_score), axis=-1)  9.68 us
  transfers between devices with their start and end apart: 1, of which 1 were waited for; matrix products, arithmetic and copies ran while one was open for 32% of the time, Pallas kernels for 0%

commit v1 on v0

--- a/solution.py
+++ b/solution.py
@@ -200,7 +200,16 @@
         .reshape(tok_rows, heads_local * HEAD_DIM)
         .astype(jnp.bfloat16)
     )
-    head_rows = lax.all_to_all(mixed, "tp", split_axis=0, concat_axis=1, tiled=True)
+
+    def cells_measure(vec, join_dim, along_dim):
+        local_next = lax.axis_size("tp")
+        y_new = jnp.split(vec, local_next, axis=join_dim)
+        after = jnp.stack(y_new)
+        tall = lax.all_to_all(after, "tp", 0, 0)
+        mid_arr = jnp.concatenate(tall, axis=along_dim)
+        return mid_arr
+
+    head_rows = cells_measure(mixed, 0, 1)
     return jnp.dot(head_rows, out_weight, preferred_element_type=jnp.float32).astype(jnp.bfloat16)
 
 

time: 280 us -> 269 us (0.961); the launches traced: 276 us -> 268 us
  local copies, waits for them, and re-layouts: 84.3 us -> 59.1 us
  waiting for transfers between devices: 7.81 us -> 28.7 us
  other arithmetic: 62.4 us -> 57.7 us
    all_gather x1, waiting for transfers between devices: 7.79 us -> 28.7 us  [per_device(): piece = lax.all_gather(kv_sel, 'kv', axis=1, tiled=True)]
    reshape x2, local copies, waits for them, and re-layouts: 17.8 us -> 5.43 us  [summarize(): blocked = blocked.reshape(kv_local, block_count, CMP_BLOCK * HEAD_DIM)]
    mul x4 -> x0, local copies, waits for them, and re-layouts: 7.9 us -> none  [the longest x2 5.26 us: per_device(): gate_cmp[..., None] * out_cmp + gate_sel[..., None] * out_sel]
    reshape x2 -> x0, local copies, waits for them, and re-layouts: 4.14 us -> none  [the longest x1 2.4 us: per_device(): out_cmp.transpose(1, 0, 2, 3).reshape(tok_rows, heads_local, HEAD_DIM)]
    convert_element_type x1, other arithmetic: 4.54 us -> 0.98 us  [per_device(): mixed = (gate_cmp[..., None] * out_cmp + gate_sel[..., None] * out_sel).r...]
  transfers between devices with their start and end apart: 1 -> 1, of which waited for: 1 -> 1; matrix products, arithmetic and copies ran while one was open for 32% -> 25% of each run, Pallas kernels for 0% -> 0%
where the time goes in v1:
time: 269 us; the launch traced here: 268 us
  local copies, waits for them, and re-layouts  59.1 us (22%)
  other arithmetic  57.7 us (21%)
  matrix products  57.4 us (21%)
  blocking collectives  51.5 us (19%)
  waiting for transfers between devices  28.7 us (11%)
  between operations  13.7 us (5%)
    all_gather x1, blocking collectives, per_device(): summaries = lax.all_gather(summary, 'kv', axis=1, tiled=True)  34.3 us
    all_gather x1, waiting for transfers between devices, per_device(): piece = lax.all_gather(kv_sel, 'kv', axis=1, tiled=True)  28.7 us
    sub x1, other arithmetic, per_device(): jax.nn.softmax(jnp.where(allowed_keys, sel_scores, masked_score), axis=-1)  24.3 us
    all_to_all x1, blocking collectives, cells_measure(): tall = lax.all_to_all(after, 'tp', 0, 0)  17.2 us
    gather x2, local copies, waits for them, and re-layouts, per_device(): fetched = blocked[head_lane, clipped]  13 us
    dot_general x1, matrix products, per_device(): jnp.dot(normed, joined_weight, preferred_element_type=jnp.float32)  12.4 us
    convert_element_type x4, local copies, waits for them, and re-layouts, summarize(): blocked = raw_rows.reshape(block_count, CMP_BLOCK, kv_local, HEAD_DIM).tr...  12 us
    sub x1, matrix products, per_device(): jax.nn.softmax(jnp.where(usable, cmp_scores, masked_score), axis=-1)  10.7 us
  transfers between devices with their start and end apart: 1, of which 1 were waited for; matrix products, arithmetic and copies ran while one was open for 25% of the time, Pallas kernels for 0%

profile of v1, /device:TPU:0, one launch (start us, length us, event | category | flops | bytes accessed | tf_op | source)
XLA Modules:
  0.0 268.1 jit_solution(14101893366955559044)
XLA Ops:
  6.6 0.7 convert_element_type.93
  7.3 5.1 %fusion.2 = f32[2048]{0:T(1024)S(1)} fusion(bf16[2048,2048]{1,0:T(8,128)(2,1)} %param.16), kind=kLoop, calls=%fused_computation.8 | loop fusion | flops 12580864 | bytes 8396800 | tf_op jit(solution)/shard_map/reduce_sum | solution.py:78
  12.4 0.9 dynamic-slice_bitcast_fusion
  13.9 1.0 multiply_cosine_fusion
  14.9 1.3 copy.87
  16.2 1.3 copy.89
  17.5 6.3 %concatenate.30 = bf16[2048,776]{1,0:T(8,128)(2,1)} concatenate(bf16[2048,256]{1,0:T(8,128)(2,1)S(1)} %copy-done.7, bf16[2048,128]{1,0:T(8,128)(2,1)} %param.19, bf16[2048,128]{1,0:T(8,128)(2,1)} %param.20, bf16[2048,128]{1,0:T(8,128)(2,1)} %param.21, bf16[2048,128]{1,0:T(8,128)(2,1)} %param.22, bf16[2048,4]{1,0:T(8,128)(2,1)S(1)} %copy.74, bf16[2048,4]{1,0:T(8,128)(2,1)S(1)} %copy.75), dimensions={1} | concatenate | bytes 6356992 | tf_op jit(solution)/shard_map/concatenate | solution.py:86
  23.8 12.4 %fusion.90 = (bf16[2048,776]{0,1:T(8,128)(2,1)S(1)}, f32[2048,776]{0,1:T(8,128)}) fusion(bf16[2048,776]{1,0:T(8,128)(2,1)} %concatenate.30, bf16[2048,2048]{1,0:T(8,128)(2,1)} %param.16, f32[2048]{0:T(1024)S(1)} %convert_element_type.93, f32[2048]{0:T(1024)S(1)} %add_rsqrt_fusion), kind=kOutput, calls=%fused_computation.141 | convolution fusion | flops 6527926272 | bytes 21118976 | tf_op jit(solution)/shard_map/dot_general | solution.py:98
  36.2 1.5 slice_convert_fusion.1
  38.2 1.3 split.52
  39.7 1.9 copy.107
  41.6 2.0 copy.106
  43.5 3.3 %subtract_convert_fusion = (bf16[2048,2,32]{2,0,1:T(8,128)(2,1)S(1)}, bf16[2048,2,32]{2,0,1:T(8,128)(2,1)S(1)}) fusion(f32[2048,2,32]{2,0,1:T(8,128)} %copy.107, f32[2048,2,32]{2,0,1:T(8,128)} %copy.106, f32[2048,32]{1,0:T(8,128)} %copy.89, f32[2048,32]{1,0:T(8,128)} %copy.87), kind=kLoop, calls=%fused_computation.47 | loop fusion | flops 1048576 | bytes 2097152 | tf_op jit(solution)/shard_map/convert.5
  46.9 1.0 copy-done.2
  47.9 1.9 fusion.108
  49.9 2.8 %split.79 = bf16[2048,256]{0,1:T(8,128)(2,1)} slice(f32[2048,776]{0,1:T(8,128)} %get-tuple-element.29), slice={[0:2048], [0:256]} | slice | bytes 2097152 | tf_op jit(solution)/shard_map/split | solution.py:115
  52.7 3.1 %split.50 = f32[2048,256]{0,1:T(8,128)} slice(f32[2048,776]{0,1:T(8,128)} %get-tuple-element.29), slice={[0:2048], [0:256]} | slice | bytes 4194304 | tf_op jit(solution)/shard_map/split | solution.py:115
  56.9 2.6 copy.76
  59.5 3.5 %reshape.280 = f32[64,32,2,64]{3,2,1,0:T(2,128)} reshape(f32[2048,128]{1,0:T(8,128)} %copy.76) | data formatting | bytes 2097152 | tf_op jit(solution)/shard_map/convert_element_type | solution.py:36
  62.9 2.8 %fusion.29 = bf16[2,64,32,64]{3,2,1,0:T(8,128)(2,1)} fusion(f32[64,32,2,64]{3,2,1,0:T(2,128)} %reshape.280, f32[2,32,64]{2,1,0:T(8,128)S(1)} %convert_element_type.100), kind=kLoop, calls=%fused_computation.45 | loop fusion | flops 524288 | bytes 1589248 | tf_op jit(solution)/shard_map/convert_element_type | solution.py:38
  65.7 2.7 %reshape.268 = bf16[2,64,2048]{2,1,0:T(8,128)(2,1)} reshape(bf16[2,64,32,64]{3,2,1,0:T(8,128)(2,1)} %fusion.29) | data formatting | bytes 1048576 | tf_op jit(solution)/shard_map/reshape | solution.py:39
  68.4 2.5 copy.78
  71.0 3.4 %reshape.281 = f32[64,32,2,64]{3,2,1,0:T(2,128)} reshape(f32[2048,128]{1,0:T(8,128)} %copy.78) | data formatting | bytes 2097152 | tf_op jit(solution)/shard_map/convert_element_type | solution.py:36
  74.4 2.8 %fusion.28 = bf16[2,64,32,64]{3,2,1,0:T(8,128)(2,1)} fusion(f32[64,32,2,64]{3,2,1,0:T(2,128)} %reshape.281, f32[2,32,64]{2,1,0:T(8,128)S(1)} %convert_element_type.107), kind=kLoop, calls=%fused_computation.43 | loop fusion | flops 524288 | bytes 1589248 | tf_op jit(solution)/shard_map/convert_element_type | solution.py:38
  77.1 2.7 %reshape.269 = bf16[2,64,2048]{2,1,0:T(8,128)(2,1)} reshape(bf16[2,64,32,64]{3,2,1,0:T(8,128)(2,1)} %fusion.28) | data formatting | bytes 1048576 | tf_op jit(solution)/shard_map/reshape | solution.py:39
  79.9 1.9 subtract_convert_fusion.1
  82.2 1.0 copy.85
  83.2 1.9 pad_maximum_fusion.1
  85.1 1.6 copy.94
  86.8 1.5 convolution_convert_fusion.2
  88.2 1.6 convolution_convert_fusion.1
  90.0 34.3 %all_gather.6 = bf16[2,512,128]{2,1,0:T(8,128)(2,1)S(1)} all-gather(bf16[2,64,128]{2,1,0:T(8,128)(2,1)S(1)} %pad_maximum_fusion.3), channel_id=1, replica_groups=mesh['kv'=8,'tp'=4] {'kv'}, dimensions={1}, use_global_device_ids=true | all-gather | bytes 294912 | tf_op jit(solution)/shard_map/all_gather | solution.py:134
  124.3 1.0 fusion.61
  125.3 2.7 %broadcast_compare_fusion = pred[2,16,128,640]{3,2,1,0:T(8,128)(4,1)} fusion(s32[16,128]{1,0:T(8,128)S(1)} %add_add_fusion, s32[2,16,640]{2,1,0:T(8,128)S(1)} %pad_add_fusion), kind=kLoop, calls=%fused_computation.29 | loop fusion | flops 2621440 | bytes 2711552 | tf_op jit(solution)/shard_map/le | solution.py:189
  128.0 2.8 %fusion.88 = (f32[2048,512]{0,1:T(8,128)}, pred[2048,512]{0,1:T(8,128)(4,1)S(1)}) fusion(s32[2048]{0:T(1024)S(1)} %get-tuple-element.34, s32[512]{0:T(512)S(1)} %multiply_add_fusion), kind=kLoop, calls=%fused_computation.139 | loop fusion | flops 2097152 | bytes 5253120 | tf_op jit(solution)/shard_map/convert_element_type | solution.py:147
  130.7 10.7 %fusion.92 = (f32[2,2048,2]{1,2,0:T(2,128)S(1)}, f32[2,2048,2,512]{1,3,2,0:T(8,128)}) fusion(pred[2048,512]{0,1:T(8,128)(4,1)S(1)} %get-tuple-element.25, bf16[2,2048,2,64]{1,3,2,0:T(8,128)(2,1)} %bitcast.142, bf16[2,512,128]{2,1,0:T(8,128)(2,1)S(1)} %all_gather.6), kind=kOutput, calls=%fused_computation.143 | convolution fusion | flops 553648640 | bytes 19169280 | tf_op jit(solution)/shard_map/sub | solution.py:145
  141.4 9.7 %fusion.18 = f32[2,2048,2,64]{1,3,2,0:T(8,128)} fusion(f32[2,2048,2,512]{1,3,2,0:T(8,128)} %get-tuple-element.33, f32[2048,512]{0,1:T(8,128)} %get-tuple-element.24, f32[2,2048,2]{1,2,0:T(2,128)S(1)} %get-tuple-element.32, bf16[2,512,128]{2,1,0:T(8,128)(2,1)S(1)} %all_gather.6), kind=kOutput, calls=%fused_computation.26 | convolution fusion | flops 549453824 | bytes 23363584 | tf_op jit(solution)/shard_map/ktgc,kcd->ktgd/dot_general | solution.py:148
  151.2 28.7 %all-gather.2.cloned.1.call-done = bf16[2,16384,128]{2,1,0:T(8,128)(2,1)} async-done(((bf16[2,2048,128]{2,1,0:T(8,128)(2,1)}), bf16[2,16384,128]{2,1,0:T(8,128)(2,1)}) %all-gather.2.cloned.1.call-update) | async-done | bytes 8388624 | tf_op jit(solution)/shard_map/all_gather | solution.py:161
  179.9 6.7 %gather_fusion = bf16[256,64,128]{2,1,0:T(8,128)(2,1)} fusion(bf16[2,256,64,128]{3,2,1,0:T(8,128)(2,1)} %bitcast.138, s32[256]{0:T(256)S(1)} %reshape.282), kind=kCustom, calls=%fused_computation | custom fusion | bytes 8390656 | tf_op jit(solution)/shard_map/gather | solution.py:166
  186.6 6.3 %copy.93 = bf16[2,16,512,128]{2,3,1,0:T(8,128)(2,1)} copy(bf16[2,16,512,128]{3,2,1,0:T(8,128)(2,1)} %bitcast.131) | data formatting | bytes 8388608 | tf_op jit(solution)/shard_map/gather | solution.py:166
  192.9 2.6 broadcast_select_fusion
  195.5 8.6 %fusion.21 = f32[2,16,128,2,640]{4,2,3,1,0:T(8,128)} fusion(bf16[2,16,128,128]{2,3,1,0:T(8,128)(2,1)S(1)} %copy.94, bf16[2,16,512,128]{2,3,1,0:T(8,128)(2,1)S(1)} %broadcast_select_fusion, bf16[16,128,2,2,32]{1,4,3,0,2:T(8,128)(2,1)S(1)} %copy-done.6, bf16[16,128,2,2,32]{1,4,3,0,2:T(8,128)(2,1)S(1)} %copy.84), kind=kOutput, calls=%fused_computation.34 | convolution fusion | flops 678428672 | bytes 27262976 | tf_op jit(solution)/shard_map/knqgd,knmd->knqgm/dot_general | solution.py:184
  204.0 24.3 %fusion.91 = (f32[2,16,128,2]{2,3,1,0:T(2,128)S(1)}, f32[2,16,128,2,640]{4,2,3,1,0:T(8,128)}) fusion(f32[2,16,128,2,640]{4,2,3,1,0:T(8,128)} %fusion.21, pred[2,16,128,640]{3,2,1,0:T(8,128)(4,1)S(1)} %copy-done.4), kind=kOutput, calls=%fused_computation.142 | output fusion | flops 31457920 | bytes 44597248 | tf_op jit(solution)/shard_map/sub | solution.py:190
  228.4 9.1 %fusion.32 = f32[16,128,2,2,64]{1,4,3,0,2:T(8,128)S(1)} fusion(bf16[2,16,512,128]{2,3,1,0:T(8,128)(2,1)S(1)} %broadcast_select_fusion, bf16[2,16,128,128]{2,3,1,0:T(8,128)(2,1)S(1)} %copy.94, f32[2,16,128,2,640]{4,2,3,1,0:T(8,128)} %get-tuple-element.31, f32[2,16,128,2]{2,3,1,0:T(2,128)S(1)} %get-tuple-element.30), kind=kOutput, calls=%fused_computation.50 | convolution fusion | flops 686817280 | bytes 28344320 | tf_op jit(solution)/shard_map/knqgm,knmd->knqgd/dot_general | solution.py:191
  237.5 1.2 copy.95
  239.1 1.0 fusion.27
  240.3 17.2 %all_to_all.5 = bf16[4,512,256]{1,2,0:T(8,128)(2,1)S(1)} all-to-all(bf16[4,512,256]{1,2,0:T(8,128)(2,1)S(1)} %pad_maximum_fusion.2), channel_id=1, replica_groups=mesh['kv'=8,'tp'=4] {'tp'}, dimensions={0} | all-to-all | bytes 2097152 | tf_op jit(solution)/shard_map/all_to_all | solution.py:208
  257.5 3.8 %convolution_convert_fusion = bf16[512,2048]{1,0:T(8,128)(2,1)} fusion(bf16[512,1024]{0,1:T(8,128)(2,1)S(1)} %bitcast.143, bf16[1024,2048]{1,0:T(8,128)(2,1)S(1)} %copy-done.11), kind=kOutput, calls=%fused_computation.31 | convolution fusion | flops 2148532224 | bytes 7340032 | tf_op jit(solution)/shard_map/dot_general | solution.py:213
  (63 shorter events, 3.3 us)
Async XLA Ops:
  6.5 80.2 %copy-start = (bf16[2,2048,64]{1,2,0:T(8,128)(2,1)S(1)}, bf16[2,2048,64]{1,2,0:T(8,128)(2,1)}, u32[]{:S(2)}) copy-start(bf16[2,2048,64]{1,2,0:T(8,128)(2,1)} %param.25) | copy-start | bytes 1572868
  6.5 173.3 %all-gather.2.cloned.1.call-start = ((), (), s32[]{:S(2)}) async-start(), calls=%async_computation.1 | async-start | bytes 9437184 | tf_op jit(solution)/shard_map/all_gather | solution.py:161
  12.4 5.2 %copy-start.7 = (bf16[2048,256]{1,0:T(8,128)(2,1)S(1)}, bf16[2048,256]{1,0:T(8,128)(2,1)}, u32[]{:S(2)}) copy-start(bf16[2048,256]{1,0:T(8,128)(2,1)} %param.18) | copy-start | bytes 3145732
  46.9 1.1 copy-start.2
  49.9 6.0 %copy-start.8 = (bf16[2,32,64]{2,1,0:T(8,128)(2,1)S(1)}, bf16[2,32,64]{2,1,0:T(8,128)(2,1)}, u32[]{:S(2)}) copy-start(bf16[2,32,64]{2,1,0:T(8,128)(2,1)} %param.24) | copy-start | bytes 24580
  49.9 6.0 %copy-start.9 = (bf16[2,32,64]{2,1,0:T(8,128)(2,1)S(1)}, bf16[2,32,64]{2,1,0:T(8,128)(2,1)}, u32[]{:S(2)}) copy-start(bf16[2,32,64]{2,1,0:T(8,128)(2,1)} %param.27) | copy-start | bytes 24580
  49.9 6.0 %copy-start.10 = (s32[2,128,8]{1,2,0:T(8,128)S(1)}, s32[2,128,8]{1,2,0:T(8,128)}, u32[]{:S(2)}) copy-start(s32[2,128,8]{1,2,0:T(8,128)} %param.31) | copy-start | bytes 24580
  79.9 3.3 %copy-start.3 = (bf16[2048,2,32]{2,0,1:T(8,128)(2,1)S(1)}, bf16[2048,2,32]{2,0,1:T(8,128)(2,1)}, u32[]{:S(2)}) copy-start(bf16[2048,2,32]{2,0,1:T(8,128)(2,1)} %copy-done.2) | copy-start | bytes 786436
  82.1 4.7 %copy-start.12 = (bf16[2,64,64]{2,1,0:T(8,128)(2,1)S(1)}, bf16[2,64,64]{2,1,0:T(8,128)(2,1)}, u32[]{:S(2)}) copy-start(bf16[2,64,64]{2,1,0:T(8,128)(2,1)} %param.26) | copy-start | bytes 49156
  82.2 6.0 %copy-start.13 = (bf16[2,64,64]{2,1,0:T(8,128)(2,1)S(1)}, bf16[2,64,64]{2,1,0:T(8,128)(2,1)}, u32[]{:S(2)}) copy-start(bf16[2,64,64]{2,1,0:T(8,128)(2,1)} %param.29) | copy-start | bytes 49156
  192.9 2.6 copy-start.6
  195.5 8.6 %copy-start.4 = (pred[2,16,128,640]{3,2,1,0:T(8,128)(4,1)S(1)}, pred[2,16,128,640]{3,2,1,0:T(8,128)(4,1)}, u32[]{:S(2)}) copy-start(pred[2,16,128,640]{3,2,1,0:T(8,128)(4,1)} %broadcast_compare_fusion) | copy-start | bytes 7864324
  237.5 1.6 copy-start.5
  240.1 17.4 %copy-start.11 = (bf16[1024,2048]{1,0:T(8,128)(2,1)S(1)}, bf16[1024,2048]{1,0:T(8,128)(2,1)}, u32[]{:S(2)}) copy-start(bf16[1024,2048]{1,0:T(8,128)(2,1)} %param.30) | copy-start | bytes 12582916
  257.5 3.8 %copy-start.1 = (bf16[2,2048,64]{1,2,0:T(8,128)(2,1)S(1)}, bf16[2,2048,64]{1,2,0:T(8,128)(2,1)}, u32[]{:S(2)}) copy-start(bf16[2,2048,64]{1,2,0:T(8,128)(2,1)} %param.25) | copy-start | bytes 1572868
Sparse Core Ops, SparseCore 0:
  50.1 129.7 all-gather.1
